TPU v7x, 32 devices: a whole 2x2x4 slice. The times are simulated.
32 devices in a mesh: sp: 16 (over z, y, core), tp: 2 (over x).
Axes of the slice: x: 2, y: 2, z: 4, core: 2. Of those that a mesh axis runs over, the one named last changes fastest.
Arguments:
- tokens: bfloat16 [16384, 2048], P('sp'), may hold values from -6 to 6
- norm_gain: float32 [2048], replicated, may hold values from 0.1 to 1.9
- w_query: bfloat16 [2048, 512], P(None, 'tp'), may hold values from -0.79549513 to 0.79549513
- w_key: bfloat16 [2048, 128], P('sp'), may hold values from -0.79549513 to 0.79549513
- w_value: bfloat16 [2048, 128], P('sp'), may hold values from -0.125 to 0.125
- w_pool_in: bfloat16 [2048, 512], P(None, 'tp'), may hold values from -0.125 to 0.125
- sink_logit: float32 [8], P('tp'), may hold values from 3 to 7
- pool_scale: float32 [512], P('tp'), may hold values from 0.05 to 0.5
- w_out: bfloat16 [1024, 2048], P('tp', 'sp'), may hold values from -0.75 to 0.75
Outputs:
- mixed_out: bfloat16 [16384, 2048], P(('sp', 'tp'))
All inputs are finite; a program needn't handle non-finite values.
Results may differ from a plain program's by a relative error of at most 0.03.
The roundings to bfloat16 on the way count: a program that leaves them out, or rounds other values in their place, can miss the bound.
Values may be sent and summed in bfloat16 or wider, within the bound.
A program may use at most 64 MiB of HBM per device.

v0:
```python
import jax
import jax.numpy as jnp
from jax import lax
from jax.sharding import PartitionSpec as P

HEAD = 64
QH = 8
KVH = 2
POOL_CH = 128
WINDOW = 128
QB = 128
NEG_BIG = -1e30
POOL_SPANS = (2, 4, 8, 16)


def extended(block, sides, width):
    for axis, dim in sides:
        count = lax.axis_size(axis)
        forward = [(i, i + 1) for i in range(count - 1)]
        backward = [(target, source) for source, target in forward]
        low = lax.ppermute(
            lax.slice_in_dim(block, block.shape[dim] - width, None, axis=dim), axis, forward
        )
        high = lax.ppermute(lax.slice_in_dim(block, 0, width, axis=dim), axis, backward)
        block = jnp.concatenate([low, block, high], axis=dim)
    return block


def layer_normed(tokens, norm_gain):
    values = tokens.astype(jnp.float32)
    center = jnp.mean(values, axis=-1, keepdims=True)
    spread = jnp.mean(jnp.square(values - center), axis=-1, keepdims=True)
    return ((values - center) * lax.rsqrt(spread + 1e-06) * norm_gain).astype(jnp.bfloat16)


def rotate(values, positions):
    half = HEAD // 2
    inverse = 10000.0 ** (-jnp.arange(half, dtype=jnp.float32) / half)
    angles = positions[:, None] * inverse[None, :]
    cosine = jnp.cos(angles)[:, None, :]
    sine = jnp.sin(angles)[:, None, :]
    first = values[..., :half]
    second = values[..., half:]
    return jnp.concatenate(
        [first * cosine - second * sine, first * sine + second * cosine], axis=-1
    )


def body(tokens, norm_gain, w_query, w_key, w_value, w_pool_in, sink_logit, pool_scale, w_out):
    local_rows = tokens.shape[0]
    seq_total = local_rows * lax.axis_size("sp")
    offset = lax.axis_index("sp") * local_rows
    tp_place = lax.axis_index("tp")
    local_heads = w_query.shape[1] // HEAD
    local_pool = w_pool_in.shape[1]
    reach = POOL_SPANS[-1] // 2
    normed = layer_normed(tokens, norm_gain)
    positions = (offset + jnp.arange(local_rows)).astype(jnp.float32)
    query = rotate(
        jnp.dot(normed, w_query, preferred_element_type=jnp.float32).reshape(
            local_rows, local_heads, HEAD
        ),
        positions,
    ).astype(jnp.bfloat16)
    key_head = tp_place * local_heads // (QH // KVH)
    key_cols = lax.dynamic_slice_in_dim(w_key, key_head * HEAD, HEAD, 1)
    value_cols = lax.dynamic_slice_in_dim(w_value, key_head * HEAD, HEAD, 1)
    key_sum = jnp.dot(
        normed,
        lax.all_gather(key_cols, "sp", axis=0, tiled=True),
        preferred_element_type=jnp.float32,
    )
    value_sum = jnp.dot(
        normed,
        lax.all_gather(value_cols, "sp", axis=0, tiled=True),
        preferred_element_type=jnp.float32,
    )
    key = rotate(key_sum[:, None, :], positions)[:, 0, :].astype(jnp.bfloat16)
    value = value_sum.astype(jnp.bfloat16)
    key_value = jnp.concatenate([key, value], axis=1)
    pool_in = jnp.dot(normed, w_pool_in, preferred_element_type=jnp.float32).astype(jnp.bfloat16)
    widened = extended(jnp.concatenate([key_value, pool_in], axis=1), (("sp", 0),), WINDOW)
    kv_wide = widened[:, : 2 * HEAD]
    pool_wide = widened[WINDOW - reach : WINDOW + local_rows + reach, 2 * HEAD :]
    span = QB + 2 * WINDOW
    sink_here = sink_logit[:, None, None]
    results = []
    for block in range(local_rows // QB):
        queries = query[block * QB : (block + 1) * QB]
        keys = kv_wide[block * QB : block * QB + span, :HEAD]
        values = kv_wide[block * QB : block * QB + span, HEAD:]
        scores = jnp.einsum(
            "ihd,jd->hij", queries, keys, preferred_element_type=jnp.float32
        ) * HEAD ** (-0.5)
        query_pos = offset + block * QB + jnp.arange(QB)
        key_pos = offset + block * QB - WINDOW + jnp.arange(span)
        valid = (
            (jnp.abs(query_pos[:, None] - key_pos[None, :]) <= WINDOW)
            & (key_pos[None, :] >= 0)
            & (key_pos[None, :] < seq_total)
        )
        scores = jnp.where(valid, scores, NEG_BIG)
        highest = jnp.maximum(jnp.max(scores, axis=-1, keepdims=True), sink_here)
        expo = jnp.where(valid, jnp.exp(scores - highest), 0.0)
        total = jnp.sum(expo, axis=-1, keepdims=True) + jnp.exp(sink_here - highest)
        weights = (expo / total).astype(jnp.bfloat16)
        result = jnp.einsum("hij,jd->ihd", weights, values, preferred_element_type=jnp.float32)
        results.append(result.reshape(QB, local_heads * HEAD).astype(jnp.bfloat16))
    attended = jnp.concatenate(results, axis=0)
    pool_vals = pool_wide.astype(jnp.float32)
    window_sum = pool_vals
    global_pos = offset + jnp.arange(local_rows)
    channel = tp_place * local_pool + jnp.arange(local_pool)
    window_group = channel // POOL_CH
    measured = jnp.zeros((local_rows, local_pool), jnp.float32)
    stride = 1
    for index, width in enumerate(POOL_SPANS):
        window_sum = window_sum[:-stride] + window_sum[stride:]
        stride = width
        sums = window_sum[reach - width // 2 : reach - width // 2 + local_rows]
        counted = (
            jnp.minimum(global_pos + width // 2, seq_total)
            - jnp.maximum(global_pos - width // 2, 0)
        ).astype(jnp.float32)
        measured = measured + jnp.where(
            window_group[None, :] == index, sums / counted[:, None], 0.0
        )
    pooled = ((measured - pool_vals[reach : reach + local_rows]) * pool_scale).astype(jnp.bfloat16)
    attended_rows, pooled_rows = (
        lax.all_to_all(attended, "tp", split_axis=0, concat_axis=1, tiled=True),
        lax.all_to_all(pooled, "tp", split_axis=0, concat_axis=1, tiled=True),
    )
    joined = jnp.concatenate([attended_rows, pooled_rows], axis=1)
    out_rows_all = lax.all_gather(w_out, "tp", axis=0, tiled=True)
    projected = jnp.dot(
        joined,
        lax.all_gather(out_rows_all, "sp", axis=1, tiled=True),
        preferred_element_type=jnp.float32,
    )
    return projected.astype(jnp.bfloat16)


def solution(mesh):
    in_specs = (
        P("sp", None),
        P(),
        P(None, "tp"),
        P("sp", None),
        P("sp", None),
        P(None, "tp"),
        P("tp"),
        P("tp"),
        P("tp", "sp"),
    )
    out_specs = P(("sp", "tp"), None)
    return jax.shard_map(body, mesh=mesh, in_specs=in_specs, out_specs=out_specs, check_vma=False)
```

profile of v0, /device:TPU:0, one launch (start us, length us, event | category | flops | bytes accessed | tf_op | source)
XLA Modules:
  0.0 166.7 jit_solution(2030448479956947112)
XLA Ops:
  7.5 24.6 %all_gather.12 = bf16[2048,64]{1,0:T(8,128)(2,1)S(1)} all-gather(bf16[128,64]{1,0:T(8,128)(2,1)S(1)} %constant_dynamic-slice_fusion.1), channel_id=1, replica_groups=mesh['sp'=16,'tp'=2] {'sp'}, dimensions={0}, use_global_device_ids=true | all-gather | bytes 278528 | tf_op jit(solution)/shard_map/all_gather | solution.py:70
  32.1 3.0 %convert_reduce_fusion = f32[1024]{0:T(1024)S(1)} fusion(bf16[1024,2048]{1,0:T(8,128)(2,1)} %param.9), kind=kLoop, calls=%fused_computation.1 | loop fusion | flops 4193280 | bytes 4198400 | tf_op jit(solution)/shard_map/reduce_sum | solution.py:31
  36.9 18.9 %all_gather.13 = bf16[2048,64]{1,0:T(8,128)(2,1)S(1)} all-gather(bf16[128,64]{1,0:T(8,128)(2,1)S(1)} %constant_dynamic-slice_fusion), channel_id=1, replica_groups=mesh['sp'=16,'tp'=2] {'sp'}, dimensions={0}, use_global_device_ids=true | all-gather | bytes 278528 | tf_op jit(solution)/shard_map/all_gather | solution.py:75
  55.8 3.0 %fusion.4 = bf16[1024,2048]{1,0:T(8,128)(2,1)S(1)} fusion(bf16[1024,2048]{1,0:T(8,128)(2,1)} %param.9, f32[2048]{0:T(1024)S(1)} %copy-done.53, f32[1024]{0:T(1024)S(1)} %add_rsqrt_fusion, f32[1024]{0:T(1024)S(1)} %broadcast_multiply_fusion), kind=kLoop, calls=%fused_computation.6 | loop fusion | flops 10485760 | bytes 8404992 | tf_op jit(solution)/shard_map/convert_element_type | solution.py:33
  58.8 1.4 convolution_bitcast_fusion
  60.2 1.4 convolution_convert_fusion.2
  64.9 3.7 %collective-permute-start = (bf16[128,384]{0,1:T(8,128)(2,1)S(1)}, bf16[128,384]{0,1:T(8,128)(2,1)}, u32[]{:S(2)}, u32[]{:S(2)}) collective-permute-start(bf16[128,384]{0,1:T(8,128)(2,1)S(1)} %get-tuple-element.9), channel_id=1, source_target_pairs={{0,2},{2,4},{4,6},{6,8},{8,10},{10,12},{12,14},{14,16},{16,18},{18... | collective-permute-start | bytes 294920 | tf_op jit(solution)/shard_map/ppermute | solution.py:21
  68.5 7.3 %all_gather.14 = bf16[1024,128]{1,0:T(8,128)(2,1)} all-gather(bf16[512,128]{1,0:T(8,128)(2,1)S(1)} %copy-done.28), channel_id=1, replica_groups=mesh['sp'=16,'tp'=2] {'tp'}, dimensions={0}, use_global_device_ids=true | all-gather | bytes 393216 | tf_op jit(solution)/shard_map/all_gather | solution.py:134
  77.9 3.8 %fusion.164 = f32[1024,256]{0,1:T(8,128)S(1)} fusion(bf16[1024,2048]{1,0:T(8,128)(2,1)} %copy-done.2, bf16[2048,256]{1,0:T(8,128)(2,1)} %param.11), kind=kOutput, calls=%fused_computation.317 | convolution fusion | flops 1073741824 | bytes 6291456 | tf_op jit(solution)/shard_map/dot_general | solution.py:60
  82.1 1.7 %fusion.163 = (f32[4,128]{1,0:T(4,128)}, f32[4,128,384]{1,2,0:T(8,128)}) fusion(bf16[1024,4,32]{0,2,1:T(8,128)(2,1)S(1)} %get-tuple-element.6, bf16[1024,4,32]{0,2,1:T(8,128)(2,1)S(1)} %get-tuple-element.5, bf16[1024,1,32]{0,2,1:T(8,128)(2,1)S(1)} %get-tuple-element.11, bf16[1024,1,32]{0,2,1:T(8,128)(2,1)S(1)} %get-tuple-element.12, ...), kind=kOutput, calls=%fused_computation.316 | convolution fusion | flops 25984512 | bytes 1492992 | tf_op jit(solution)/shard_map/ihd,jd->hij/dot_general | solution.py:92
  84.0 1.8 %fusion.162 = (f32[4,128]{1,0:T(4,128)}, f32[4,128,384]{1,2,0:T(8,128)}) fusion(bf16[1024,4,32]{0,2,1:T(8,128)(2,1)S(1)} %get-tuple-element.6, bf16[1024,4,32]{0,2,1:T(8,128)(2,1)S(1)} %get-tuple-element.5, bf16[1024,1,32]{0,2,1:T(8,128)(2,1)S(1)} %get-tuple-element.11, bf16[1024,1,32]{0,2,1:T(8,128)(2,1)S(1)} %get-tuple-element.12, ...), kind=kOutput, calls=%fused_computation.315 | convolution fusion | flops 25984512 | bytes 1492992 | tf_op jit(solution)/shard_map/ihd,jd->hij/dot_general | solution.py:92
  86.1 1.8 %fusion.161 = (f32[4,128]{1,0:T(4,128)}, f32[4,128,384]{1,2,0:T(8,128)}) fusion(bf16[1024,4,32]{0,2,1:T(8,128)(2,1)S(1)} %get-tuple-element.6, bf16[1024,4,32]{0,2,1:T(8,128)(2,1)S(1)} %get-tuple-element.5, bf16[1024,1,32]{0,2,1:T(8,128)(2,1)S(1)} %get-tuple-element.11, bf16[1024,1,32]{0,2,1:T(8,128)(2,1)S(1)} %get-tuple-element.12, ...), kind=kOutput, calls=%fused_computation.314 | convolution fusion | flops 25984512 | bytes 1492992 | tf_op jit(solution)/shard_map/ihd,jd->hij/dot_general | solution.py:92
  88.1 1.8 %fusion.160 = (f32[4,128]{1,0:T(4,128)}, f32[4,128,384]{1,2,0:T(8,128)}) fusion(bf16[1024,4,32]{0,2,1:T(8,128)(2,1)S(1)} %get-tuple-element.6, bf16[1024,4,32]{0,2,1:T(8,128)(2,1)S(1)} %get-tuple-element.5, bf16[1024,1,32]{0,2,1:T(8,128)(2,1)S(1)} %get-tuple-element.11, bf16[1024,1,32]{0,2,1:T(8,128)(2,1)S(1)} %get-tuple-element.12, ...), kind=kOutput, calls=%fused_computation.313 | convolution fusion | flops 25984512 | bytes 1492992 | tf_op jit(solution)/shard_map/ihd,jd->hij/dot_general | solution.py:92
  90.1 1.8 %fusion.159 = (f32[4,128]{1,0:T(4,128)}, f32[4,128,384]{1,2,0:T(8,128)}) fusion(bf16[1024,4,32]{0,2,1:T(8,128)(2,1)S(1)} %get-tuple-element.6, bf16[1024,4,32]{0,2,1:T(8,128)(2,1)S(1)} %get-tuple-element.5, bf16[1024,1,32]{0,2,1:T(8,128)(2,1)S(1)} %get-tuple-element.11, bf16[1024,1,32]{0,2,1:T(8,128)(2,1)S(1)} %get-tuple-element.12, ...), kind=kOutput, calls=%fused_computation.312 | convolution fusion | flops 25984512 | bytes 1492992 | tf_op jit(solution)/shard_map/ihd,jd->hij/dot_general | solution.py:92
  92.1 1.7 %fusion.158 = (f32[4,128]{1,0:T(4,128)}, f32[4,128,384]{1,2,0:T(8,128)}) fusion(bf16[1024,4,32]{0,2,1:T(8,128)(2,1)S(1)} %get-tuple-element.6, bf16[1024,4,32]{0,2,1:T(8,128)(2,1)S(1)} %get-tuple-element.5, bf16[1024,1,32]{0,2,1:T(8,128)(2,1)S(1)} %get-tuple-element.11, bf16[1024,1,32]{0,2,1:T(8,128)(2,1)S(1)} %get-tuple-element.12, ...), kind=kOutput, calls=%fused_computation.311 | convolution fusion | flops 25984512 | bytes 1492992 | tf_op jit(solution)/shard_map/ihd,jd->hij/dot_general | solution.py:92
  98.4 1.6 convolution_convert_fusion.3
  100.1 1.6 copy.42
  107.3 1.6 copy.41
  108.9 1.6 convolution_convert_fusion.5
  110.5 1.6 copy.40
  112.1 2.1 %convolution_convert_fusion.6 = bf16[64,4,128]{2,0,1:T(8,128)(2,1)} fusion(f32[4,128,384]{1,2,0:T(8,128)} %get-tuple-element.42, f32[4,128]{1,0:T(4,128)} %get-tuple-element.29, f32[4,128]{1,0:T(4,128)} %get-tuple-element.20, pred[128,384]{0,1:T(8,128)(4,1)S(1)} %fusion.52, bf16[1024,64]{0,1:T(8,128)(2,1)S(1)} %convolution_convert_fusion.2), kind=kOutput, calls=%fused_computation.41 | convolution fusion | flops 25985024 | bytes 954368 | tf_op jit(solution)/shard_map/hij,jd->ihd/dot_general | solution.py:107
  114.2 1.6 copy.39
  115.8 1.6 convolution_convert_fusion.7
  117.4 1.6 copy.38
  119.0 2.1 %convolution_convert_fusion.8 = bf16[64,4,128]{2,0,1:T(8,128)(2,1)} fusion(f32[4,128,384]{1,2,0:T(8,128)} %get-tuple-element.38, f32[4,128]{1,0:T(4,128)S(1)} %copy-done.58, f32[4,128]{1,0:T(4,128)S(1)} %copy-done.51, pred[128,384]{0,1:T(8,128)(4,1)S(1)} %copy-done.14, bf16[1024,64]{0,1:T(8,128)(2,1)S(1)} %convolution_convert_fusion.2), kind=kOutput, calls=%fused_computation.43 | convolution fusion | flops 25985024 | bytes 954368 | tf_op jit(solution)/shard_map/hij,jd->ihd/dot_general | solution.py:107
  121.1 1.6 copy.37
  130.9 3.7 %all-to-all-start = ((bf16[2,512,256]{2,1,0:T(8,128)(2,1)}), bf16[2,512,256]{2,1,0:T(8,128)(2,1)S(1)}, u32[]{:S(2)}, u32[]{:S(2)}) async-start(bf16[2,512,256]{2,1,0:T(8,128)(2,1)} %bitcast.49), calls=%async_computation | async-start | bytes 1048576 | tf_op jit(solution)/shard_map/all_to_all | solution.py:130
  137.7 1.6 fusion.22
  140.2 2.7 %all-to-all-done = bf16[2,512,256]{2,1,0:T(8,128)(2,1)S(1)} async-done(((bf16[2,512,256]{2,1,0:T(8,128)(2,1)}), bf16[2,512,256]{2,1,0:T(8,128)(2,1)S(1)}, u32[]{:S(2)}, u32[]{:S(2)}) %all-to-all-start) | async-done | bytes 524320 | tf_op jit(solution)/shard_map/all_to_all | solution.py:130
  142.9 3.5 %all-to-all-start.1 = ((bf16[2,512,256]{1,2,0:T(8,128)(2,1)}), bf16[2,512,256]{1,2,0:T(8,128)(2,1)S(1)}, u32[]{:S(2)}, u32[]{:S(2)}) async-start(bf16[2,512,256]{1,2,0:T(8,128)(2,1)} %bitcast.149), calls=%async_computation.1 | async-start | bytes 1048576 | tf_op jit(solution)/shard_map/all_to_all | solution.py:131
  146.6 7.4 %all-to-all-done.1 = bf16[2,512,256]{1,2,0:T(8,128)(2,1)S(1)} async-done(((bf16[2,512,256]{1,2,0:T(8,128)(2,1)}), bf16[2,512,256]{1,2,0:T(8,128)(2,1)S(1)}, u32[]{:S(2)}, u32[]{:S(2)}) %all-to-all-start.1) | async-done | bytes 524320 | tf_op jit(solution)/shard_map/all_to_all | solution.py:131
  154.0 5.9 %convolution_convert_fusion = bf16[512,2048]{1,0:T(8,128)(2,1)} fusion(bf16[1024,2048]{1,0:T(8,128)(2,1)} %all-gather.2.cloned.1.call-done, bf16[512,512]{0,1:T(8,128)(2,1)S(1)} %bitcast.153, bf16[512,512]{0,1:T(8,128)(2,1)S(1)} %bitcast.154), kind=kOutput, calls=%fused_computation.7 | convolution fusion | flops 2150629376 | bytes 7340032 | tf_op jit(solution)/shard_map/dot_general | solution.py:135
  (216 shorter events, 31.3 us)
Async XLA Ops:
  6.5 55.1 %copy-start = (bf16[2048,256]{1,0:T(8,128)(2,1)S(1)}, bf16[2048,256]{1,0:T(8,128)(2,1)}, u32[]{:S(2)}) copy-start(bf16[2048,256]{1,0:T(8,128)(2,1)} %param.14) | copy-start | bytes 3145732
  6.5 147.5 %all-gather.2.cloned.1.call-start = ((), (), s32[]{:S(2)}) async-start(), calls=%async_computation.2 | async-start | bytes 4456448 | tf_op jit(solution)/shard_map/all_gather | solution.py:137
  35.5 20.2 %copy-start.53 = (f32[2048]{0:T(1024)S(1)}, f32[2048]{0:T(1024)}, u32[]{:S(2)}) copy-start(f32[2048]{0:T(1024)} %param.10) | copy-start | bytes 24580
  61.6 6.9 %copy-start.28 = (bf16[512,128]{1,0:T(8,128)(2,1)S(1)}, bf16[512,128]{1,0:T(8,128)(2,1)}, u32[]{:S(2)}) copy-start(bf16[512,128]{1,0:T(8,128)(2,1)} %param.17) | copy-start | bytes 393220
  63.6 31.9 %collective-permute-start.1 = (bf16[128,384]{0,1:T(8,128)(2,1)S(1)}, bf16[128,384]{0,1:T(8,128)(2,1)S(1)}, u32[]{:S(2)}, u32[]{:S(2)}) collective-permute-start(bf16[128,384]{0,1:T(8,128)(2,1)S(1)} %get-tuple-element.10), channel_id=1, source_target_pairs={{2,0},{4,2},{6,4},{8,6},{10,8},{12,10},{14,12},{16,14},{18,16},{20... | collective-permute-start | bytes 294920 | tf_op jit(solution)/shard_map/ppermute | solution.py:24
  64.9 31.0 %collective-permute-start = (bf16[128,384]{0,1:T(8,128)(2,1)S(1)}, bf16[128,384]{0,1:T(8,128)(2,1)}, u32[]{:S(2)}, u32[]{:S(2)}) collective-permute-start(bf16[128,384]{0,1:T(8,128)(2,1)S(1)} %get-tuple-element.9), channel_id=1, source_target_pairs={{0,2},{2,4},{4,6},{6,8},{8,10},{10,12},{12,14},{14,16},{16,18},{18... | collective-permute-start | bytes 294920 | tf_op jit(solution)/shard_map/ppermute | solution.py:21
  88.1 5.7 %copy-start.10 = (pred[128,384]{0,1:T(8,128)(4,1)}, pred[128,384]{0,1:T(8,128)(4,1)S(1)}, u32[]{:S(2)}) copy-start(pred[128,384]{0,1:T(8,128)(4,1)S(1)} %fusion.50) | copy-start | bytes 147460
  90.1 5.7 %copy-start.12 = (pred[128,384]{0,1:T(8,128)(4,1)}, pred[128,384]{0,1:T(8,128)(4,1)S(1)}, u32[]{:S(2)}) copy-start(pred[128,384]{0,1:T(8,128)(4,1)S(1)} %fusion.48) | copy-start | bytes 147460
  92.1 4.8 %copy-start.15 = (pred[128,384]{0,1:T(8,128)(4,1)}, pred[128,384]{0,1:T(8,128)(4,1)S(1)}, u32[]{:S(2)}) copy-start(pred[128,384]{0,1:T(8,128)(4,1)S(1)} %fusion.46) | copy-start | bytes 147460
  97.7 4.0 %copy-start.4 = (f32[4,128,384]{1,2,0:T(8,128)S(1)}, f32[4,128,384]{1,2,0:T(8,128)}, u32[]{:S(2)}) copy-start(f32[4,128,384]{1,2,0:T(8,128)} %get-tuple-element.44) | copy-start | bytes 2359300
  101.7 3.6 %copy-start.8 = (f32[4,128,384]{1,2,0:T(8,128)S(1)}, f32[4,128,384]{1,2,0:T(8,128)}, u32[]{:S(2)}) copy-start(f32[4,128,384]{1,2,0:T(8,128)} %get-tuple-element.36) | copy-start | bytes 2359300
  101.7 3.6 %copy-start.16 = (pred[128,384]{0,1:T(8,128)(4,1)S(1)}, pred[128,384]{0,1:T(8,128)(4,1)}, u32[]{:S(2)}) copy-start(pred[128,384]{0,1:T(8,128)(4,1)} %copy-done.15) | copy-start | bytes 147460
  101.7 3.6 %copy-start.48 = (f32[4,128]{1,0:T(4,128)S(1)}, f32[4,128]{1,0:T(4,128)}, u32[]{:S(2)}) copy-start(f32[4,128]{1,0:T(4,128)} %get-tuple-element.17) | copy-start | bytes 6148
  101.7 3.8 %copy-start.3 = (f32[4,128,384]{1,2,0:T(8,128)S(1)}, f32[4,128,384]{1,2,0:T(8,128)}, u32[]{:S(2)}) copy-start(f32[4,128,384]{1,2,0:T(8,128)} %get-tuple-element.46) | copy-start | bytes 2359300
  101.7 3.8 %copy-start.52 = (f32[4,128]{1,0:T(4,128)S(1)}, f32[4,128]{1,0:T(4,128)}, u32[]{:S(2)}) copy-start(f32[4,128]{1,0:T(4,128)} %get-tuple-element.22) | copy-start | bytes 6148
  110.5 5.3 %copy-start.6 = (f32[4,128,384]{1,2,0:T(8,128)S(1)}, f32[4,128,384]{1,2,0:T(8,128)}, u32[]{:S(2)}) copy-start(f32[4,128,384]{1,2,0:T(8,128)} %get-tuple-element.40) | copy-start | bytes 2359300
  110.5 5.3 %copy-start.11 = (pred[128,384]{0,1:T(8,128)(4,1)S(1)}, pred[128,384]{0,1:T(8,128)(4,1)}, u32[]{:S(2)}) copy-start(pred[128,384]{0,1:T(8,128)(4,1)} %copy-done.10) | copy-start | bytes 147460
  114.2 4.8 %copy-start.14 = (pred[128,384]{0,1:T(8,128)(4,1)S(1)}, pred[128,384]{0,1:T(8,128)(4,1)}, u32[]{:S(2)}) copy-start(pred[128,384]{0,1:T(8,128)(4,1)} %copy-done.12) | copy-start | bytes 147460
  114.2 4.8 %copy-start.51 = (f32[4,128]{1,0:T(4,128)S(1)}, f32[4,128]{1,0:T(4,128)}, u32[]{:S(2)}) copy-start(f32[4,128]{1,0:T(4,128)} %get-tuple-element.18) | copy-start | bytes 6148
  114.2 4.8 %copy-start.58 = (f32[4,128]{1,0:T(4,128)S(1)}, f32[4,128]{1,0:T(4,128)}, u32[]{:S(2)}) copy-start(f32[4,128]{1,0:T(4,128)} %get-tuple-element.27) | copy-start | bytes 6148
  117.4 5.3 %copy-start.9 = (f32[4,128,384]{1,2,0:T(8,128)S(1)}, f32[4,128,384]{1,2,0:T(8,128)}, u32[]{:S(2)}) copy-start(f32[4,128,384]{1,2,0:T(8,128)} %get-tuple-element.36) | copy-start | bytes 2359300
  117.4 5.3 %copy-start.17 = (pred[128,384]{0,1:T(8,128)(4,1)S(1)}, pred[128,384]{0,1:T(8,128)(4,1)}, u32[]{:S(2)}) copy-start(pred[128,384]{0,1:T(8,128)(4,1)} %copy-done.15) | copy-start | bytes 147460
  117.4 5.3 %copy-start.49 = (f32[4,128]{1,0:T(4,128)S(1)}, f32[4,128]{1,0:T(4,128)}, u32[]{:S(2)}) copy-start(f32[4,128]{1,0:T(4,128)} %get-tuple-element.17) | copy-start | bytes 6148
  117.4 5.3 %copy-start.57 = (f32[4,128]{1,0:T(4,128)S(1)}, f32[4,128]{1,0:T(4,128)}, u32[]{:S(2)}) copy-start(f32[4,128]{1,0:T(4,128)} %get-tuple-element.26) | copy-start | bytes 6148
  121.1 3.5 %copy-start.56 = (f32[4,128]{1,0:T(4,128)S(1)}, f32[4,128]{1,0:T(4,128)}, u32[]{:S(2)}) copy-start(f32[4,128]{1,0:T(4,128)} %get-tuple-element.16) | copy-start | bytes 6148
  124.6 3.8 %copy-start.25 = (bf16[128,256]{1,0:T(8,128)(2,1)S(1)}, bf16[128,256]{1,0:T(8,128)(2,1)}, u32[]{:S(2)}) copy-start(bf16[128,256]{1,0:T(8,128)(2,1)} %copy.39) | copy-start | bytes 196612
  124.6 4.4 %copy-start.24 = (bf16[128,256]{1,0:T(8,128)(2,1)S(1)}, bf16[128,256]{1,0:T(8,128)(2,1)}, u32[]{:S(2)}) copy-start(bf16[128,256]{1,0:T(8,128)(2,1)} %copy.40) | copy-start | bytes 196612
  124.7 5.0 %copy-start.23 = (bf16[128,256]{1,0:T(8,128)(2,1)S(1)}, bf16[128,256]{1,0:T(8,128)(2,1)}, u32[]{:S(2)}) copy-start(bf16[128,256]{1,0:T(8,128)(2,1)} %copy.41) | copy-start | bytes 196612
  124.7 5.6 %copy-start.22 = (bf16[128,256]{1,0:T(8,128)(2,1)S(1)}, bf16[128,256]{1,0:T(8,128)(2,1)}, u32[]{:S(2)}) copy-start(bf16[128,256]{1,0:T(8,128)(2,1)} %copy.42) | copy-start | bytes 196612
  124.7 9.9 %copy-start.21 = (bf16[128,384]{0,1:T(8,128)(2,1)S(1)}, bf16[128,384]{0,1:T(8,128)(2,1)}, u32[]{:S(2)}) copy-start(bf16[128,384]{0,1:T(8,128)(2,1)} %copy-done.20) | copy-start | bytes 294916
  130.9 12.0 %all-to-all-start = ((bf16[2,512,256]{2,1,0:T(8,128)(2,1)}), bf16[2,512,256]{2,1,0:T(8,128)(2,1)S(1)}, u32[]{:S(2)}, u32[]{:S(2)}) async-start(bf16[2,512,256]{2,1,0:T(8,128)(2,1)} %bitcast.49), calls=%async_computation | async-start | bytes 1048576 | tf_op jit(solution)/shard_map/all_to_all | solution.py:130
  142.9 11.1 %all-to-all-start.1 = ((bf16[2,512,256]{1,2,0:T(8,128)(2,1)}), bf16[2,512,256]{1,2,0:T(8,128)(2,1)S(1)}, u32[]{:S(2)}, u32[]{:S(2)}) async-start(bf16[2,512,256]{1,2,0:T(8,128)(2,1)} %bitcast.149), calls=%async_computation.1 | async-start | bytes 1048576 | tf_op jit(solution)/shard_map/all_to_all | solution.py:131
  (37 other events, 77.8 us)
Sparse Core Ops, SparseCore 0:
  76.0 49.8 all-gather.1
where the time goes:
time: 168 us; the launch traced here: 167 us
  blocking collectives  50.8 us (30%)
  matrix products  37.6 us (22%)
  other arithmetic  22.2 us (13%)
  local copies, waits for them, and re-layouts  19.4 us (12%)
  between operations  14.5 us (9%)
  starting transfers between devices  12.2 us (7%)
  waiting for transfers between devices  10.2 us (6%)
    all_gather x1, blocking collectives, body(): lax.all_gather(key_cols, 'sp', axis=0, tiled=True)  24.6 us
    all_gather x1, blocking collectives, body(): lax.all_gather(value_cols, 'sp', axis=0, tiled=True)  18.9 us
    dot_general x8, matrix products, body(): jnp.einsum('hij,jd->ihd', weights, values, preferred_element_type=jnp.flo...  11.9 us
    dot_general x8, matrix products, body(): jnp.einsum('ihd,jd->hij', queries, keys, preferred_element_type=jnp.float32)  11.9 us
    convert_element_type x8, local copies, waits for them, and re-layouts, body(): results.append(result.reshape(QB, local_heads * HEAD).astype(jnp.bfloat16))  10.6 us
    all_to_all x1, waiting for transfers between devices, body(): lax.all_to_all(pooled, 'tp', split_axis=0, concat_axis=1, tiled=True)  7.42 us
    all_gather x1, blocking collectives, body(): out_rows_all = lax.all_gather(w_out, 'tp', axis=0, tiled=True)  7.31 us
    dot_general x1, matrix products, body(): jnp.dot(joined, lax.all_gather(out_rows_all, 'sp', axis=1, tiled=True), p...  5.88 us
  transfers between devices with their start and end apart: 5, of which 2 were waited for; matrix products, arithmetic and copies ran while one was open for 35% of the time, Pallas kernels for 0%

commit v1 on v0

--- a/solution.py
+++ b/solution.py
@@ -128,7 +128,10 @@
     pooled = ((measured - pool_vals[reach : reach + local_rows]) * pool_scale).astype(jnp.bfloat16)
     attended_rows, pooled_rows = (
         lax.all_to_all(attended, "tp", split_axis=0, concat_axis=1, tiled=True),
-        lax.all_to_all(pooled, "tp", split_axis=0, concat_axis=1, tiled=True),
+        jnp.concatenate(
+            lax.all_to_all(jnp.stack(jnp.split(pooled, lax.axis_size("tp"), axis=0)), "tp", 0, 0),
+            axis=1,
+        ),
     )
     joined = jnp.concatenate([attended_rows, pooled_rows], axis=1)
     out_rows_all = lax.all_gather(w_out, "tp", axis=0, tiled=True)

time: 168 us -> 146 us (0.87)
  local copies, waits for them, and re-layouts: 19.4 us -> 4.6 us
  matrix products: 37.6 us -> 26 us
  blocking collectives: 50.8 us -> 60.9 us
  waiting for transfers between devices: 10.2 us -> 3.73 us
  other arithmetic: 22.2 us -> 27.1 us
  starting transfers between devices: 12.2 us -> 8.44 us
    convert_element_type x8 -> x0, local copies, waits for them, and re-layouts: 10.6 us -> none  [body(): results.append(result.reshape(QB, local_heads * HEAD).astype(jnp.bfloat16))]
    all_to_all x0 -> x1, blocking collectives: none -> 10.2 us  [body(): lax.all_to_all(jnp.stack(jnp.split(pooled, lax.axis_size('tp'), axis=0)),...]
    dot_general x8, matrix products: 11.9 us -> 4.02 us  [body(): jnp.einsum('hij,jd->ihd', weights, values, preferred_element_type=jnp.flo...]
    all_to_all x1 -> x0, waiting for transfers between devices: 7.42 us -> none  [body(): lax.all_to_all(pooled, 'tp', split_axis=0, concat_axis=1, tiled=True)]
    dot_general x8, matrix products: 11.9 us -> 8.27 us  [body(): jnp.einsum('ihd,jd->hij', queries, keys, preferred_element_type=jnp.float32)]
    all_to_all x1 -> x0, starting transfers between devices: 3.49 us -> none  [body(): lax.all_to_all(pooled, 'tp', split_axis=0, concat_axis=1, tiled=True)]
    lt x8, other arithmetic: 0.06 us -> 3.48 us  [body(): key_pos[None, :] < seq_total]
    unnamed x135 -> x73, local copies, waits for them, and re-layouts: 5.75 us -> 2.33 us
  transfers between devices with their start and end apart: 5 -> 4, of which waited for: 2 -> 1; matrix products, arithmetic and copies ran while one was open for 35% -> 25% of each run, Pallas kernels for 0% -> 0%
where the time goes in v1:
time: 146 us; the launch traced here: 145 us
  blocking collectives  60.9 us (42%)
  other arithmetic  27.1 us (19%)
  matrix products  26 us (18%)
  between operations  14.1 us (10%)
  starting transfers between devices  8.44 us (6%)
  local copies, waits for them, and re-layouts  4.6 us (3%)
  waiting for transfers between devices  3.73 us (3%)
    all_gather x1, blocking collectives, body(): lax.all_gather(key_cols, 'sp', axis=0, tiled=True)  24.6 us
    all_gather x1, blocking collectives, body(): lax.all_gather(value_cols, 'sp', axis=0, tiled=True)  18.9 us
    all_to_all x1, blocking collectives, body(): lax.all_to_all(jnp.stack(jnp.split(pooled, lax.axis_size('tp'), axis=0)),...  10.2 us
    dot_general x8, matrix products, body(): jnp.einsum('ihd,jd->hij', queries, keys, preferred_element_type=jnp.float32)  8.27 us
    all_gather x1, blocking collectives, body(): out_rows_all = lax.all_gather(w_out, 'tp', axis=0, tiled=True)  7.31 us
    dot_general x1, matrix products, body(): jnp.dot(joined, lax.all_gather(out_rows_all, 'sp', axis=1, tiled=True), p...  5.88 us
    dot_general x8, matrix products, body(): jnp.einsum('hij,jd->ihd', weights, values, preferred_element_type=jnp.flo...  4.02 us
    dot_general x1, matrix products, body(): jnp.dot(normed, w_query, preferred_element_type=jnp.float32)  3.78 us
  transfers between devices with their start and end apart: 4, of which 1 were waited for; matrix products, arithmetic and copies ran while one was open for 25% of the time, Pallas kernels for 0%

profile of v1, /device:TPU:0, one launch (start us, length us, event | category | flops | bytes accessed | tf_op | source)
XLA Modules:
  0.0 144.9 jit_solution(8550265951908007729)
XLA Ops:
  6.6 0.9 constant_dynamic-slice_fusion.1
  7.5 24.6 %all_gather.12 = bf16[2048,64]{1,0:T(8,128)(2,1)S(1)} all-gather(bf16[128,64]{1,0:T(8,128)(2,1)S(1)} %constant_dynamic-slice_fusion.1), channel_id=1, replica_groups=mesh['sp'=16,'tp'=2] {'sp'}, dimensions={0}, use_global_device_ids=true | all-gather | bytes 278528 | tf_op jit(solution)/shard_map/all_gather | solution.py:70
  32.1 3.0 %convert_reduce_fusion = f32[1024]{0:T(1024)S(1)} fusion(bf16[1024,2048]{1,0:T(8,128)(2,1)} %param.9), kind=kLoop, calls=%fused_computation.1 | loop fusion | flops 4193280 | bytes 4198400 | tf_op jit(solution)/shard_map/reduce_sum | solution.py:31
  35.5 1.2 fusion.2
  36.9 18.9 %all_gather.13 = bf16[2048,64]{1,0:T(8,128)(2,1)S(1)} all-gather(bf16[128,64]{1,0:T(8,128)(2,1)S(1)} %constant_dynamic-slice_fusion), channel_id=1, replica_groups=mesh['sp'=16,'tp'=2] {'sp'}, dimensions={0}, use_global_device_ids=true | all-gather | bytes 278528 | tf_op jit(solution)/shard_map/all_gather | solution.py:75
  55.8 3.0 %fusion.4 = bf16[1024,2048]{1,0:T(8,128)(2,1)S(1)} fusion(bf16[1024,2048]{1,0:T(8,128)(2,1)} %param.9, f32[2048]{0:T(1024)S(1)} %copy-done.14, f32[1024]{0:T(1024)S(1)} %add_rsqrt_fusion, f32[1024]{0:T(1024)S(1)} %broadcast_multiply_fusion), kind=kLoop, calls=%fused_computation.6 | loop fusion | flops 10485760 | bytes 8404992 | tf_op jit(solution)/shard_map/convert_element_type | solution.py:33
  58.8 1.4 convolution_bitcast_fusion
  60.2 1.4 convolution_convert_fusion.2
  61.6 1.3 convolution_convert_fusion.1
  63.5 0.7 pad_maximum_fusion.8
  64.2 1.3 collective-permute-start.1
  65.5 3.7 %collective-permute-start = (bf16[128,384]{0,1:T(8,128)(2,1)}, bf16[128,384]{0,1:T(8,128)(2,1)}, u32[]{:S(2)}, u32[]{:S(2)}) collective-permute-start(bf16[128,384]{0,1:T(8,128)(2,1)} %get-tuple-element.9), channel_id=1, source_target_pairs={{0,2},{2,4},{4,6},{6,8},{8,10},{10,12},{12,14},{14,16},{16,18},{18... | collective-permute-start | bytes 294920 | tf_op jit(solution)/shard_map/ppermute | solution.py:21
  69.2 7.3 %all_gather.14 = bf16[1024,128]{1,0:T(8,128)(2,1)} all-gather(bf16[512,128]{1,0:T(8,128)(2,1)S(1)} %copy-done.10), channel_id=1, replica_groups=mesh['sp'=16,'tp'=2] {'tp'}, dimensions={0}, use_global_device_ids=true | all-gather | bytes 393216 | tf_op jit(solution)/shard_map/all_gather | solution.py:137
  85.2 3.8 %fusion.164 = f32[1024,256]{0,1:T(8,128)S(1)} fusion(bf16[1024,2048]{1,0:T(8,128)(2,1)} %copy-done.2, bf16[2048,256]{1,0:T(8,128)(2,1)} %param.11), kind=kOutput, calls=%fused_computation.320 | convolution fusion | flops 1073741824 | bytes 6291456 | tf_op jit(solution)/shard_map/dot_general | solution.py:60
  90.0 1.2 fusion.162
  91.4 1.2 fusion.161
  92.9 1.2 fusion.160
  94.3 1.2 fusion.159
  96.3 1.2 fusion.158
  98.1 0.9 fusion.58
  99.0 0.9 fusion.44
  100.5 1.0 fusion.156
  101.5 1.0 fusion.157
  103.0 1.2 convolution_convert_fusion.10
  108.1 1.0 convolution_convert_fusion.3
  109.2 0.8 copy.29
  110.0 3.5 %all-to-all-start = ((bf16[2,512,256]{1,2,0:T(8,128)(2,1)}), bf16[2,512,256]{1,2,0:T(8,128)(2,1)S(1)}, u32[]{:S(2)}, u32[]{:S(2)}) async-start(bf16[2,512,256]{1,2,0:T(8,128)(2,1)} %bitcast.153), calls=%async_computation | async-start | bytes 1048576 | tf_op jit(solution)/shard_map/all_to_all | solution.py:130
  113.5 1.1 fusion.42
  116.5 1.6 %fusion.22 = bf16[1024,256]{0,1:T(8,128)(2,1)S(1)} fusion(f32[1040,256]{0,1:T(8,128)S(1)} %fusion.42, f32[1025,256]{0,1:T(8,128)S(1)} %get-tuple-element.8, f32[1025,256]{0,1:T(8,128)S(1)} %get-tuple-element.7, f32[1033,256]{0,1:T(8,128)S(1)} %slice_add_fusion, f32[1037,256]{0,1:T(8,128)S(1)} %slice_add_fusion.1, f32[1039,256]{0,1:T(8,128)S(1)} %slice_add_fusion.2, ...), kind=kLoop, calls=%fused_computation.48 | loop fusion | flops 3932160 | bytes 6834176 | tf_op jit(solution)/shard_map/convert_element_type | solution.py:128
  118.3 3.7 %all-to-all-done = bf16[2,512,256]{1,2,0:T(8,128)(2,1)S(1)} async-done(((bf16[2,512,256]{1,2,0:T(8,128)(2,1)}), bf16[2,512,256]{1,2,0:T(8,128)(2,1)S(1)}, u32[]{:S(2)}, u32[]{:S(2)}) %all-to-all-start) | async-done | bytes 524320 | tf_op jit(solution)/shard_map/all_to_all | solution.py:130
  122.0 10.2 %all_to_all.24 = bf16[2,512,256]{1,2,0:T(8,128)(2,1)S(1)} all-to-all(bf16[2,512,256]{1,2,0:T(8,128)(2,1)S(1)} %pad_maximum_fusion.4), channel_id=1, replica_groups=mesh['sp'=16,'tp'=2] {'tp'}, dimensions={0} | all-to-all | bytes 1048576 | tf_op jit(solution)/shard_map/all_to_all | solution.py:132
  132.2 5.9 %convolution_convert_fusion = bf16[512,2048]{1,0:T(8,128)(2,1)} fusion(bf16[1024,2048]{1,0:T(8,128)(2,1)} %all-gather.2.cloned.1.call-done, bf16[512,512]{0,1:T(8,128)(2,1)S(1)} %bitcast.157, bf16[512,512]{0,1:T(8,128)(2,1)S(1)} %bitcast.156), kind=kOutput, calls=%fused_computation.7 | convolution fusion | flops 2150629376 | bytes 7340032 | tf_op jit(solution)/shard_map/dot_general | solution.py:138
  (146 shorter events, 19.5 us)
Async XLA Ops:
  6.5 55.1 %copy-start = (bf16[2048,256]{1,0:T(8,128)(2,1)S(1)}, bf16[2048,256]{1,0:T(8,128)(2,1)}, u32[]{:S(2)}) copy-start(bf16[2048,256]{1,0:T(8,128)(2,1)} %param.14) | copy-start | bytes 3145732
  6.5 125.7 %all-gather.2.cloned.1.call-start = ((), (), s32[]{:S(2)}) async-start(), calls=%async_computation.2 | async-start | bytes 4456448 | tf_op jit(solution)/shard_map/all_gather | solution.py:140
  32.1 3.4 %copy-start.1 = (bf16[1024,2048]{1,0:T(8,128)(2,1)S(1)}, bf16[1024,2048]{1,0:T(8,128)(2,1)}, u32[]{:S(2)}) copy-start(bf16[1024,2048]{1,0:T(8,128)(2,1)} %param.9) | copy-start | bytes 12582916
  35.5 1.3 copy-start.11
  35.5 20.2 %copy-start.14 = (f32[2048]{0:T(1024)S(1)}, f32[2048]{0:T(1024)}, u32[]{:S(2)}) copy-start(f32[2048]{0:T(1024)} %param.10) | copy-start | bytes 24580
  58.8 2.8 %copy-start.2 = (bf16[1024,2048]{1,0:T(8,128)(2,1)}, bf16[1024,2048]{1,0:T(8,128)(2,1)S(1)}, u32[]{:S(2)}) copy-start(bf16[1024,2048]{1,0:T(8,128)(2,1)S(1)} %fusion.4) | copy-start | bytes 12582916
  61.6 7.6 %copy-start.10 = (bf16[512,128]{1,0:T(8,128)(2,1)S(1)}, bf16[512,128]{1,0:T(8,128)(2,1)}, u32[]{:S(2)}) copy-start(bf16[512,128]{1,0:T(8,128)(2,1)} %param.17) | copy-start | bytes 393220
  64.2 36.2 %collective-permute-start.1 = (bf16[128,384]{0,1:T(8,128)(2,1)}, bf16[128,384]{0,1:T(8,128)(2,1)}, u32[]{:S(2)}, u32[]{:S(2)}) collective-permute-start(bf16[128,384]{0,1:T(8,128)(2,1)} %get-tuple-element.10), channel_id=1, source_target_pairs={{2,0},{4,2},{6,4},{8,6},{10,8},{12,10},{14,12},{16,14},{18,16},{20... | collective-permute-start | bytes 294920 | tf_op jit(solution)/shard_map/ppermute | solution.py:24
  65.5 35.9 %collective-permute-start = (bf16[128,384]{0,1:T(8,128)(2,1)}, bf16[128,384]{0,1:T(8,128)(2,1)}, u32[]{:S(2)}, u32[]{:S(2)}) collective-permute-start(bf16[128,384]{0,1:T(8,128)(2,1)} %get-tuple-element.9), channel_id=1, source_target_pairs={{0,2},{2,4},{4,6},{6,8},{8,10},{10,12},{12,14},{14,16},{16,18},{18... | collective-permute-start | bytes 294920 | tf_op jit(solution)/shard_map/ppermute | solution.py:21
  89.0 0.7 copy-start.26
  89.0 0.7 copy-start.27
  89.0 0.7 copy-start.28
  89.0 2.2 %copy-start.23 = (pred[384]{0:T(512)(128)(4,1)S(1)}, pred[384]{0:T(512)(128)(4,1)}, u32[]{:S(2)}) copy-start(pred[384]{0:T(512)(128)(4,1)} %get-tuple-element.67) | copy-start | bytes 1156
  89.0 2.2 %copy-start.24 = (pred[384]{0:T(512)(128)(4,1)S(1)}, pred[384]{0:T(512)(128)(4,1)}, u32[]{:S(2)}) copy-start(pred[384]{0:T(512)(128)(4,1)} %get-tuple-element.68) | copy-start | bytes 1156
  89.0 2.2 %copy-start.25 = (s32[128]{0:T(128)S(1)}, s32[128]{0:T(128)}, u32[]{:S(2)}) copy-start(s32[128]{0:T(128)} %iota_add_fusion.12) | copy-start | bytes 1540
  90.0 4.1 %copy-start.20 = (pred[384]{0:T(512)(128)(4,1)S(1)}, pred[384]{0:T(512)(128)(4,1)}, u32[]{:S(2)}) copy-start(pred[384]{0:T(512)(128)(4,1)} %get-tuple-element.63) | copy-start | bytes 1156
  90.0 4.1 %copy-start.21 = (pred[384]{0:T(512)(128)(4,1)S(1)}, pred[384]{0:T(512)(128)(4,1)}, u32[]{:S(2)}) copy-start(pred[384]{0:T(512)(128)(4,1)} %get-tuple-element.64) | copy-start | bytes 1156
  90.0 4.1 %copy-start.22 = (s32[128]{0:T(128)S(1)}, s32[128]{0:T(128)}, u32[]{:S(2)}) copy-start(s32[128]{0:T(128)} %iota_add_fusion.14) | copy-start | bytes 1540
  91.4 4.1 %copy-start.17 = (s32[128]{0:T(128)S(1)}, s32[128]{0:T(128)}, u32[]{:S(2)}) copy-start(s32[128]{0:T(128)} %iota_add_fusion.15) | copy-start | bytes 1540
  91.4 4.1 %copy-start.18 = (pred[384]{0:T(512)(128)(4,1)S(1)}, pred[384]{0:T(512)(128)(4,1)}, u32[]{:S(2)}) copy-start(pred[384]{0:T(512)(128)(4,1)} %get-tuple-element.53) | copy-start | bytes 1156
  91.4 4.1 %copy-start.19 = (pred[384]{0:T(512)(128)(4,1)S(1)}, pred[384]{0:T(512)(128)(4,1)}, u32[]{:S(2)}) copy-start(pred[384]{0:T(512)(128)(4,1)} %get-tuple-element.54) | copy-start | bytes 1156
  100.4 2.1 %copy-start.15 = (f32[4]{0:T(128)S(1)}, f32[4]{0:T(128)}, u32[]{:S(2)}) copy-start(f32[4]{0:T(128)} %param.15) | copy-start | bytes 52
  102.9 1.3 copy-start.3
  103.0 1.4 copy-start.4
  103.0 1.6 %copy-start.5 = (f32[4,128,384]{1,2,0:T(8,128)S(1)}, f32[4,128,384]{1,2,0:T(8,128)}, u32[]{:S(2)}) copy-start(f32[4,128,384]{1,2,0:T(8,128)} %get-tuple-element.42) | copy-start | bytes 2359300
  104.2 1.2 copy-start.6
  104.2 1.5 %copy-start.7 = (f32[4,128,384]{1,2,0:T(8,128)S(1)}, f32[4,128,384]{1,2,0:T(8,128)}, u32[]{:S(2)}) copy-start(f32[4,128,384]{1,2,0:T(8,128)} %get-tuple-element.38) | copy-start | bytes 2359300
  104.2 1.4 copy-start.9
  110.0 12.0 %all-to-all-start = ((bf16[2,512,256]{1,2,0:T(8,128)(2,1)}), bf16[2,512,256]{1,2,0:T(8,128)(2,1)S(1)}, u32[]{:S(2)}, u32[]{:S(2)}) async-start(bf16[2,512,256]{1,2,0:T(8,128)(2,1)} %bitcast.153), calls=%async_computation | async-start | bytes 1048576 | tf_op jit(solution)/shard_map/all_to_all | solution.py:130
  115.8 0.7 copy-start.12
  115.8 0.7 copy-start.13
  115.8 0.7 copy-start.16
  (5 other events, 3.3 us)
Sparse Core Ops, SparseCore 0:
  76.7 50.9 all-gather.1
